TPU v7x, 512 devices: a whole 4x8x8 slice. The times are simulated.
512 devices in a mesh: ep: 32 (over z, x), tp: 16 (over y, core).
Axes of the slice: x: 4, y: 8, z: 8, core: 2. Of those that a mesh axis runs over, the one named last changes fastest.
Arguments:
- query_rows: bfloat16 [16384, 3072], P('ep', 'tp'), may hold values from -6 to 6
- key_rows: bfloat16 [16384, 1024], P('ep', 'tp'), may hold values from -6 to 6
- value_rows: bfloat16 [16384, 1024], P('ep', 'tp'), may hold values from -6 to 6
- query_gain: float32 [48, 64], P('tp'), may hold values from 0.4 to 48
- key_gain: float32 [16, 64], P('tp'), may hold values from 0.1 to 1.9
- sink_logits: float32 [48], P('tp'), may hold values from 1 to 6
- out_weight: bfloat16 [3072, 2048], P('tp'), may hold values from -0.109375 to 0.109375
- expert_input: bfloat16 [16384, 2048], P(('ep', 'tp')), may hold values from -6 to 6
- expert_gain: float32 [2048], replicated, may hold values from 0.1 to 1.9
- routes: int32 [16384, 2], P(('ep', 'tp')), may hold values from 0 to 31, all different within a row; in each aligned block of 32 rows (0 to 31, 32 to 63, ...) at most 3 rows name the same one
- route_logits: float32 [16384, 2], P(('ep', 'tp')), may hold values from -6 to 6
- gate_weight: bfloat16 [32, 2048, 2048], P('ep', None, 'tp'), may hold values from -0.375 to 0.375
- up_weight: bfloat16 [32, 2048, 2048], P('ep', None, 'tp'), may hold values from -0.375 to 0.375
- down_weight: bfloat16 [32, 2048, 2048], P('ep', 'tp'), may hold values from -0.01953125 to 0.01953125
Outputs:
- attended: bfloat16 [16384, 2048], P(('ep', 'tp'))
- expert_mix: bfloat16 [16384, 2048], P(('ep', 'tp'))
Inputs may be any that keep to these rules, and one draw needn't show every extreme that they name: `routes`: each row names 2 different experts; in the rows of one device no expert is named more than 3 times, and in some device one expert is named exactly 3 times.
All inputs are finite; a program needn't handle non-finite values.
Results may differ from a plain program's by a relative error of at most 0.017.
The roundings to bfloat16 on the way count: a program that leaves them out, or rounds other values in their place, can miss the bound.
Values may be sent and summed in bfloat16 or wider, within the bound.
A program may use at most 64 MiB of HBM per device.

v0:
```python
import jax
import jax.numpy as jnp
from jax import lax
from jax.sharding import PartitionSpec as P

EXPERTS = 32
WINDOW = 128
EPSILON = 1e-06
CLAMP_LIMIT = 7.0
ACT_SLOPE = 1.702
NEGATIVE = -1e30


def shifted(value, axis, steps):
    count = lax.axis_size(axis)
    initial, last = (max(0, -steps), min(count, count - steps))
    return lax.ppermute(value, axis, [(source, source + steps) for source in range(initial, last)])


def head_norm(row_data, gain_table):
    head_count, head_size = gain_table.shape
    widened = row_data.astype(jnp.float32).reshape(row_data.shape[0], head_count, head_size)
    scaled = widened * lax.rsqrt(jnp.mean(widened * widened, axis=-1, keepdims=True) + EPSILON)
    return (scaled * gain_table).astype(jnp.bfloat16)


def band(padded, blocks):
    tiled = padded.reshape((blocks + 1, WINDOW) + padded.shape[1:])
    return jnp.concatenate([tiled[:-1], tiled[1:]], axis=1)


def attend(query_rows, key_rows, value_rows, query_gain, key_gain, sink_logits):
    seq_rows = query_rows.shape[0]
    key_heads, head_size = key_gain.shape
    group_size = query_gain.shape[0] // key_heads
    blocks = seq_rows // WINDOW
    query_hat = head_norm(query_rows, query_gain).reshape(
        blocks, WINDOW, key_heads, group_size, head_size
    )
    key_hat = head_norm(key_rows, key_gain)
    value_hat = value_rows.reshape(seq_rows, key_heads, head_size)
    tail_rows = jnp.stack([key_hat[seq_rows - WINDOW :], value_hat[seq_rows - WINDOW :]])
    earlier = shifted(tail_rows, "ep", 1)
    key_band = band(jnp.concatenate([earlier[0], key_hat], axis=0), blocks)
    value_band = band(jnp.concatenate([earlier[1], value_hat], axis=0), blocks)
    query_pos = lax.broadcasted_iota(jnp.int32, (WINDOW, 2 * WINDOW), 0)
    key_pos = lax.broadcasted_iota(jnp.int32, (WINDOW, 2 * WINDOW), 1)
    distance = query_pos + WINDOW - key_pos
    inside = (distance >= 0) & (distance < WINDOW)
    first_block = (lax.broadcasted_iota(jnp.int32, (blocks, 1, 1), 0) == 0) & (
        lax.axis_index("ep") == 0
    )
    allowed = inside[None] & ~(first_block & (key_pos < WINDOW)[None])
    scores = jnp.einsum(
        "bqkgd,bjkd->bkgqj", query_hat, key_band, preferred_element_type=jnp.float32
    ) * head_size ** (-0.5)
    scores = jnp.where(allowed[:, None, None], scores, NEGATIVE)
    sink_table = sink_logits.reshape(1, key_heads, group_size, 1, 1)
    highest = jnp.maximum(jnp.max(scores, axis=-1, keepdims=True), sink_table)
    weights = jnp.exp(scores - highest)
    total = jnp.sum(weights, axis=-1, keepdims=True) + jnp.exp(sink_table - highest)
    mixed = jnp.einsum(
        "bkgqj,bjkd->bkgqd",
        weights.astype(jnp.bfloat16),
        value_band,
        preferred_element_type=jnp.float32,
    )
    mixed = (mixed / total).astype(jnp.bfloat16)
    return jnp.transpose(mixed, (0, 3, 1, 2, 4)).reshape(seq_rows, -1)


def slot_maps(route_block, capacity):
    flat_routes = route_block.reshape(-1)
    expert_hot = (flat_routes[:, None] == lax.broadcasted_iota(jnp.int32, (1, EXPERTS), 1)).astype(
        jnp.int32
    )
    before = jnp.cumsum(expert_hot, axis=0) - expert_hot
    position = jnp.sum(before * expert_hot, axis=1)
    place_hot = (position[:, None] == lax.broadcasted_iota(jnp.int32, (1, capacity), 1)).astype(
        jnp.float32
    )
    row_total, fanout = route_block.shape
    return (
        expert_hot.astype(jnp.float32).reshape(row_total, fanout, EXPERTS),
        place_hot.reshape(row_total, fanout, capacity),
    )


def dispatch_matrix(route_block, capacity):
    expert_hot, place_hot = slot_maps(route_block, capacity)
    return jnp.einsum("rke,rkc->ecr", expert_hot, place_hot).astype(jnp.bfloat16)


def combine_matrix(route_block, route_weight, capacity):
    expert_hot, place_hot = slot_maps(route_block, capacity)
    return jnp.einsum("rke,rkc,rk->rec", expert_hot, place_hot, route_weight)


def expert_hidden(piece, gate_weight, up_weight):
    gate_pre = jnp.einsum("aecd,edf->aecf", piece, gate_weight, preferred_element_type=jnp.float32)
    up_pre = jnp.einsum("aecd,edf->aecf", piece, up_weight, preferred_element_type=jnp.float32)
    clipped = jnp.minimum(gate_pre, CLAMP_LIMIT)
    linear = jnp.clip(up_pre, -CLAMP_LIMIT, CLAMP_LIMIT)
    return (clipped * jax.nn.sigmoid(ACT_SLOPE * clipped) * (linear + 1.0)).astype(jnp.bfloat16)


def on_device(
    query_rows,
    key_rows,
    value_rows,
    query_gain,
    key_gain,
    sink_logits,
    out_weight,
    expert_input,
    expert_gain,
    routes,
    route_logits,
    gate_weight,
    up_weight,
    down_weight,
):
    heads_out = attend(query_rows, key_rows, value_rows, query_gain, key_gain, sink_logits)
    attended = lax.psum_scatter(
        jnp.dot(heads_out, out_weight, preferred_element_type=jnp.float32).astype(jnp.bfloat16),
        "tp",
        scatter_dimension=0,
        tiled=True,
    )
    own_rows = expert_input.shape[0]
    fanout = routes.shape[1]
    capacity = (3 * own_rows * fanout + 2 * EXPERTS - 1) // (2 * EXPERTS)
    ep_size = lax.axis_size("ep")
    tp_size = lax.axis_size("tp")
    local_experts = gate_weight.shape[0]
    widened = expert_input.astype(jnp.float32)
    normed = (
        widened
        * lax.rsqrt(jnp.mean(widened * widened, axis=-1, keepdims=True) + EPSILON)
        * expert_gain
    ).astype(jnp.bfloat16)
    route_weight = jax.nn.softmax(route_logits, axis=-1)
    combine = combine_matrix(routes, route_weight, capacity)
    sender = dispatch_matrix(routes, capacity)
    slot_rows = jnp.einsum(
        "ecr,rd->ecd", sender, normed, preferred_element_type=jnp.float32
    ).astype(jnp.bfloat16)
    slot_rows = slot_rows.reshape(ep_size, local_experts, capacity, -1)
    arrived = lax.all_to_all(slot_rows, "ep", split_axis=0, concat_axis=0, tiled=True)
    hidden_units = expert_hidden(
        lax.all_gather(arrived, "tp", axis=0, tiled=True), gate_weight, up_weight
    )
    partial_value = jnp.einsum(
        "aecf,efd->aecd", hidden_units, down_weight, preferred_element_type=jnp.float32
    ).astype(jnp.bfloat16)
    partial_value = partial_value.reshape(tp_size, ep_size * local_experts * capacity, -1)
    pieces = lax.all_to_all(partial_value, "tp", split_axis=0, concat_axis=0, tiled=True)
    summed = jnp.sum(pieces, axis=0, dtype=jnp.float32).astype(jnp.bfloat16)
    summed = summed.reshape(ep_size, local_experts * capacity, -1)
    returned = lax.all_to_all(summed, "ep", split_axis=0, concat_axis=0, tiled=True)
    expert_mix = jnp.einsum("rec,ecd->rd", combine, returned.astype(jnp.float32)).astype(
        jnp.bfloat16
    )
    return (attended, expert_mix)


def solution(mesh):
    placed = (
        P("ep", "tp"),
        P("ep", "tp"),
        P("ep", "tp"),
        P("tp", None),
        P("tp", None),
        P("tp"),
        P("tp", None),
        P(("ep", "tp"), None),
        P(),
        P(("ep", "tp"), None),
        P(("ep", "tp"), None),
        P("ep", None, "tp"),
        P("ep", None, "tp"),
        P("ep", "tp", None),
    )
    return jax.shard_map(
        on_device,
        mesh=mesh,
        in_specs=placed,
        out_specs=(P(("ep", "tp"), None), P(("ep", "tp"), None)),
        check_vma=False,
    )
```

profile of v0, /device:TPU:24, one launch (start us, length us, event | category | flops | bytes accessed | tf_op | source)
XLA Modules:
  0.0 328.0 jit_solution(9556012948772609825)
XLA Ops:
  7.2 0.0 copy-start
  7.2 0.0 all-gather.2.cloned.1.call-start
  7.2 1.1 fusion.58
  8.3 0.8 copy.42
  9.1 0.1 eq.68
  9.2 0.1 fusion.86
  9.3 0.1 reduce_window_sum.12
  9.4 0.2 select_reduce_fusion
  9.6 0.1 eq.72
  9.7 0.0 copy-start.9
  9.7 0.4 fusion.34
  10.1 1.2 fusion.4
  11.3 0.3 copy.46
  11.6 30.7 %all_to_all.15 = bf16[32,1,3,2048]{3,2,1,0:T(4,128)(2,1)S(1)} all-to-all(bf16[32,1,3,2048]{3,2,1,0:T(4,128)(2,1)S(1)} %copy.46), channel_id=1, replica_groups=mesh['ep'=32,'tp'=16] {'ep'}, dimensions={0} | all-to-all | bytes 786432 | tf_op jit(solution)/shard_map/all_to_all | solution.py:149
  42.3 1.1 copy.47
  43.4 0.0 all-gather.2.cloned.1.call-update
  43.4 0.0 copy-start.3
  43.4 0.0 copy-start.4
  43.5 44.1 %all-gather.2.cloned.1.call-done = bf16[512,1,3,2048]{3,0,2,1:T(8,128)(2,1)} async-done(((bf16[32,1,3,2048]{3,0,2,1:T(8,128)(2,1)}), bf16[512,1,3,2048]{3,0,2,1:T(8,128)(2,1)}) %all-gather.2.cloned.1.call-update) | async-done | bytes 6291472 | tf_op jit(solution)/shard_map/all_gather | solution.py:151
  87.5 4.6 %fusion.11 = f32[512,1,3,128]{3,0,2,1:T(8,128)S(1)} fusion(bf16[512,1,3,2048]{3,0,2,1:T(8,128)(2,1)} %all-gather.2.cloned.1.call-done, bf16[1,2048,128]{2,1,0:T(8,128)(2,1)S(1)} %copy-done.9), kind=kOutput, calls=%fused_computation.15 | convolution fusion | flops 805502976 | bytes 7602176 | tf_op jit(solution)/shard_map/aecd,edf->aecf/dot_general | solution.py:100
  92.1 11.9 %convert_bitcast_fusion = bf16[512,1,3,2048]{3,0,2,1:T(8,128)(2,1)} fusion(bf16[512,1,3,2048]{3,0,2,1:T(8,128)(2,1)} %all-gather.2.cloned.1.call-done, f32[512,1,3,128]{3,0,2,1:T(8,128)S(1)} %fusion.11, bf16[1,128,2048]{2,1,0:T(8,128)(2,1)S(1)} %copy-done.3, bf16[1,2048,128]{2,1,0:T(8,128)(2,1)S(1)} %copy-done.4), kind=kOutput, calls=%fused_computation.4 | convolution fusion | flops 1615527936 | bytes 14417920 | tf_op jit(solution)/shard_map/aecf,efd->aecd/dot_general | solution.py:153
  104.1 11.6 %copy.48 = bf16[512,1,3,2048]{3,2,0,1:T(4,128)(2,1)} copy(bf16[512,1,3,2048]{3,0,2,1:T(8,128)(2,1)} %convert_bitcast_fusion) | data formatting | bytes 12582912 | tf_op jit(solution)/shard_map/convert_element_type | solution.py:155
  115.6 16.3 %reshape.224 = bf16[16,96,2048]{2,1,0:T(8,128)(2,1)} reshape(bf16[512,1,3,2048]{3,2,0,1:T(4,128)(2,1)} %copy.48) | data formatting | bytes 12582912 | tf_op jit(solution)/shard_map/reshape | solution.py:156
  132.0 5.5 %all-to-all-start.1 = ((bf16[16,96,2048]{2,1,0:T(8,128)(2,1)}), bf16[16,96,2048]{2,1,0:T(8,128)(2,1)}, u32[]{:S(2)}, u32[]{:S(2)}) async-start(bf16[16,96,2048]{2,1,0:T(8,128)(2,1)} %reshape.224), calls=%async_computation.2 | async-start | bytes 12582912 | tf_op jit(solution)/shard_map/all_to_all | solution.py:157
  137.5 0.0 reduce-scatter.2.cloned.1.call-start
  137.6 0.1 fusion.68
  137.7 3.4 %collective-permute-start = (bf16[2,128,1,64]{1,3,2,0:T(8,128)(2,1)S(1)}, bf16[2,128,1,64]{1,3,2,0:T(8,128)(2,1)S(1)}, u32[]{:S(2)}, u32[]{:S(2)}) collective-permute-start(bf16[2,128,1,64]{1,3,2,0:T(8,128)(2,1)S(1)} %pad_maximum_fusion.2), channel_id=1, source_target_pairs={{0,16},{16,32},{32,48},{48,64},{64,80},{80,96},{96,112},{112,128},... | collective-permute-start | bytes 98312 | tf_op jit(solution)/shard_map/ppermute | solution.py:17
  141.2 0.0 copy-start.8
  141.3 0.1 fusion.107
  141.4 0.2 not_and_fusion
  141.6 0.1 reshape.213
  141.8 0.9 collective-permute-done
  142.7 0.5 fusion.105
  143.2 0.1 broadcast_maximum_fusion
  143.3 0.2 fusion.6
  143.5 0.1 exponential_add_fusion
  143.6 0.4 fusion.33
  144.0 0.2 copy.41
  144.1 2.1 convolution_convert_fusion
  146.2 0.0 reduce-scatter.2.cloned.1.call-update
  146.3 140.4 %all-to-all-done.1 = bf16[16,96,2048]{2,1,0:T(8,128)(2,1)} async-done(((bf16[16,96,2048]{2,1,0:T(8,128)(2,1)}), bf16[16,96,2048]{2,1,0:T(8,128)(2,1)}, u32[]{:S(2)}, u32[]{:S(2)}) %all-to-all-start.1) | async-done | bytes 6291488 | tf_op jit(solution)/shard_map/all_to_all | solution.py:157
  286.7 4.1 %reduce_sum.76 = bf16[96,2048]{1,0:T(8,128)(2,1)S(1)} reduce(bf16[16,96,2048]{2,1,0:T(8,128)(2,1)} %all-to-all-done.1, bf16[]{:T(256)} %constant.49.clone.1), dimensions={0}, to_apply=%region_10.11 | reduce | flops 2949120 | bytes 6684674 | tf_op jit(solution)/shard_map/reduce_sum | solution.py:158
  290.8 1.0 reshape.225
  291.8 10.2 %all-to-all-start.2 = ((bf16[32,3,2048]{2,1,0:T(4,128)(2,1)}), bf16[32,3,2048]{2,1,0:T(4,128)(2,1)S(1)}, u32[]{:S(2)}, u32[]{:S(2)}) async-start(bf16[32,3,2048]{2,1,0:T(4,128)(2,1)} %reshape.225), calls=%async_computation.3 | async-start | bytes 1048576 | tf_op jit(solution)/shard_map/all_to_all | solution.py:160
  302.0 0.1 copy.44
  302.2 0.4 fusion.84
  302.5 17.5 %all-to-all-done.2 = bf16[32,3,2048]{2,1,0:T(4,128)(2,1)S(1)} async-done(((bf16[32,3,2048]{2,1,0:T(4,128)(2,1)}), bf16[32,3,2048]{2,1,0:T(4,128)(2,1)S(1)}, u32[]{:S(2)}, u32[]{:S(2)}) %all-to-all-start.2) | async-done | bytes 393248 | tf_op jit(solution)/shard_map/all_to_all | solution.py:160
  320.1 1.1 fusion.5
  (40 shorter events, 0.4 us)
Async XLA Ops:
  7.2 137.0 %copy-start = (bf16[192,2048]{1,0:T(8,128)(2,1)S(1)}, bf16[192,2048]{1,0:T(8,128)(2,1)}, u32[]{:S(2)}) copy-start(bf16[192,2048]{1,0:T(8,128)(2,1)} %param.20) | copy-start | bytes 2359300
  7.2 80.4 %all-gather.2.cloned.1.call-start = ((), (), s32[]{:S(2)}) async-start(), calls=%async_computation.5 | async-start | bytes 6684672 | tf_op jit(solution)/shard_map/all_gather | solution.py:151
  9.7 77.9 %copy-start.9 = (bf16[1,2048,128]{2,1,0:T(8,128)(2,1)S(1)}, bf16[1,2048,128]{2,1,0:T(8,128)(2,1)}, u32[]{:S(2)}) copy-start(bf16[1,2048,128]{2,1,0:T(8,128)(2,1)} %param.25) | copy-start | bytes 1572868
  43.4 48.7 %copy-start.3 = (bf16[1,128,2048]{2,1,0:T(8,128)(2,1)S(1)}, bf16[1,128,2048]{2,1,0:T(8,128)(2,1)}, u32[]{:S(2)}) copy-start(bf16[1,128,2048]{2,1,0:T(8,128)(2,1)} %param.27) | copy-start | bytes 1572868
  43.4 48.7 %copy-start.4 = (bf16[1,2048,128]{2,1,0:T(8,128)(2,1)S(1)}, bf16[1,2048,128]{2,1,0:T(8,128)(2,1)}, u32[]{:S(2)}) copy-start(bf16[1,2048,128]{2,1,0:T(8,128)(2,1)} %param.26) | copy-start | bytes 1572868
  131.9 5.6 %copy-start.2 = (bf16[512,64]{0,1:T(8,128)(2,1)S(1)}, bf16[512,64]{0,1:T(8,128)(2,1)}, u32[]{:S(2)}) copy-start(bf16[512,64]{0,1:T(8,128)(2,1)} %param.15) | copy-start | bytes 196612
  132.0 5.6 %copy-start.7 = (f32[1,64]{1,0:T(1,128)S(1)}, f32[1,64]{1,0:T(1,128)}, u32[]{:S(2)}) copy-start(f32[1,64]{1,0:T(1,128)} %param.18) | copy-start | bytes 772
  132.0 5.7 %copy-start.5 = (bf16[512,64]{0,1:T(8,128)(2,1)S(1)}, bf16[512,64]{0,1:T(8,128)(2,1)}, u32[]{:S(2)}) copy-start(bf16[512,64]{0,1:T(8,128)(2,1)} %param.16) | copy-start | bytes 196612
  132.0 9.1 %copy-start.1 = (bf16[512,192]{0,1:T(8,128)(2,1)S(1)}, bf16[512,192]{0,1:T(8,128)(2,1)}, u32[]{:S(2)}) copy-start(bf16[512,192]{0,1:T(8,128)(2,1)} %param.14) | copy-start | bytes 589828
  132.0 154.7 %all-to-all-start.1 = ((bf16[16,96,2048]{2,1,0:T(8,128)(2,1)}), bf16[16,96,2048]{2,1,0:T(8,128)(2,1)}, u32[]{:S(2)}, u32[]{:S(2)}) async-start(bf16[16,96,2048]{2,1,0:T(8,128)(2,1)} %reshape.224), calls=%async_computation.2 | async-start | bytes 12582912 | tf_op jit(solution)/shard_map/all_to_all | solution.py:157
  137.5 5.3 %copy-start.10 = (f32[3,64]{1,0:T(4,128)S(1)}, f32[3,64]{1,0:T(4,128)}, u32[]{:S(2)}) copy-start(f32[3,64]{1,0:T(4,128)} %param.17) | copy-start | bytes 2308
  137.5 183.7 %reduce-scatter.2.cloned.1.call-start = ((), (), s32[]{:S(2)}) async-start(), calls=%async_computation.4 | async-start | bytes 2228224 | tf_op jit(solution)/shard_map/reduce_scatter | solution.py:124
  137.7 5.0 %collective-permute-start = (bf16[2,128,1,64]{1,3,2,0:T(8,128)(2,1)S(1)}, bf16[2,128,1,64]{1,3,2,0:T(8,128)(2,1)S(1)}, u32[]{:S(2)}, u32[]{:S(2)}) collective-permute-start(bf16[2,128,1,64]{1,3,2,0:T(8,128)(2,1)S(1)} %pad_maximum_fusion.2), channel_id=1, source_target_pairs={{0,16},{16,32},{32,48},{48,64},{64,80},{80,96},{96,112},{112,128},... | collective-permute-start | bytes 98312 | tf_op jit(solution)/shard_map/ppermute | solution.py:17
  141.2 2.0 copy-start.8
  146.3 155.7 %copy-start.6 = (f32[32,2]{0,1:T(2,128)S(1)}, f32[32,2]{0,1:T(2,128)}, u32[]{:S(2)}) copy-start(f32[32,2]{0,1:T(2,128)} %param.24) | copy-start | bytes 772
  291.8 28.3 %all-to-all-start.2 = ((bf16[32,3,2048]{2,1,0:T(4,128)(2,1)}), bf16[32,3,2048]{2,1,0:T(4,128)(2,1)S(1)}, u32[]{:S(2)}, u32[]{:S(2)}) async-start(bf16[32,3,2048]{2,1,0:T(4,128)(2,1)} %reshape.225), calls=%async_computation.3 | async-start | bytes 1048576 | tf_op jit(solution)/shard_map/all_to_all | solution.py:160
Sparse Core Ops, SparseCore 0:
  43.6 43.9 all-gather.1
  146.4 136.6 reduce-scatter.1
where the time goes:
time: 329 us; the launch traced here: 328 us
  waiting for transfers between devices  203 us (62%)
  local copies, waits for them, and re-layouts  31.8 us (10%)
  blocking collectives  30.7 us (9%)
  matrix products  22.5 us (7%)
  starting transfers between devices  19.1 us (6%)
  between operations  14.4 us (4%)
  other arithmetic  6.53 us (2%)
    all_to_all x1, waiting for transfers between devices, on_device(): lax.all_to_all(partial_value, 'tp', split_axis=0, concat_axis=0, tiled=True)  140 us
    all_gather x1, waiting for transfers between devices, on_device(): lax.all_gather(arrived, 'tp', axis=0, tiled=True)  44.1 us
    all_to_all x1, blocking collectives, on_device(): lax.all_to_all(slot_rows, 'ep', split_axis=0, concat_axis=0, tiled=True)  30.7 us
    all_to_all x1, waiting for transfers between devices, on_device(): lax.all_to_all(summed, 'ep', split_axis=0, concat_axis=0, tiled=True)  17.5 us
    reshape x1, local copies, waits for them, and re-layouts, on_device(): partial_value.reshape(tp_size, ep_size * local_experts * capacity, -1)  16.3 us
    dot_general x1, matrix products, on_device(): jnp.einsum('aecf,efd->aecd', hidden_units, down_weight, preferred_element...  11.9 us
    convert_element_type x1, local copies, waits for them, and re-layouts, on_device(): partial_value = jnp.einsum('aecf,efd->aecd', hidden_units, down_weight, p...  11.6 us
    all_to_all x1, starting transfers between devices, on_device(): lax.all_to_all(summed, 'ep', split_axis=0, concat_axis=0, tiled=True)  10.2 us
  transfers between devices with their start and end apart: 5, of which 4 were waited for; matrix products, arithmetic and copies ran while one was open for 3% of the time, Pallas kernels for 0%

commit v1 on v0

--- a/solution.py
+++ b/solution.py
@@ -2,6 +2,7 @@
 import jax.numpy as jnp
 from jax import lax
 from jax.sharding import PartitionSpec as P
+from jax.lax import all_to_all, axis_size
 
 EXPERTS = 32
 WINDOW = 128
@@ -9,6 +10,15 @@
 CLAMP_LIMIT = 7.0
 ACT_SLOPE = 1.702
 NEGATIVE = -1e30
+
+
+def show_table_here(xx, array_dim):
+    tile_out = axis_size("tp")
+    current_arr = jnp.concatenate(tile_out * [xx], axis=array_dim)
+    step_out = all_to_all(
+        current_arr, axis_name="tp", split_axis=array_dim, concat_axis=array_dim, tiled=True
+    )
+    return step_out
 
 
 def shifted(value, axis, steps):
@@ -147,9 +157,7 @@
     ).astype(jnp.bfloat16)
     slot_rows = slot_rows.reshape(ep_size, local_experts, capacity, -1)
     arrived = lax.all_to_all(slot_rows, "ep", split_axis=0, concat_axis=0, tiled=True)
-    hidden_units = expert_hidden(
-        lax.all_gather(arrived, "tp", axis=0, tiled=True), gate_weight, up_weight
-    )
+    hidden_units = expert_hidden(show_table_here(arrived, 0), gate_weight, up_weight)
     partial_value = jnp.einsum(
         "aecf,efd->aecd", hidden_units, down_weight, preferred_element_type=jnp.float32
     ).astype(jnp.bfloat16)

time: 329 us -> 484 us (1.47)
  blocking collectives: 30.7 us -> 221 us
  waiting for transfers between devices: 203 us -> 159 us
  matrix products: 22.5 us -> 29.5 us
  local copies, waits for them, and re-layouts: 31.8 us -> 38.2 us
  starting transfers between devices: 19.1 us -> 13.3 us
    all_to_all x0 -> x1, blocking collectives: none -> 191 us  [show_table_here(): all_to_all(current_arr, axis_name='tp', split_axis=array_dim, concat_axis...]
    all_gather x1 -> x0, waiting for transfers between devices: 44.1 us -> none  [on_device(): lax.all_gather(arrived, 'tp', axis=0, tiled=True)]
    unnamed x23 -> x40, local copies, waits for them, and re-layouts: 0.83 us -> 8.16 us
    all_to_all x1, starting transfers between devices: 10.2 us -> 4.64 us  [on_device(): lax.all_to_all(summed, 'ep', split_axis=0, concat_axis=0, tiled=True)]
  transfers between devices with their start and end apart: 5 -> 4, of which waited for: 4 -> 3; matrix products, arithmetic and copies ran while one was open for 3% -> 2% of each run, Pallas kernels for 0% -> 0%
where the time goes in v1:
time: 484 us; the launch traced here: 483 us
  blocking collectives  221 us (46%)
  waiting for transfers between devices  159 us (33%)
  local copies, waits for them, and re-layouts  38.2 us (8%)
  matrix products  29.5 us (6%)
  between operations  14.5 us (3%)
  starting transfers between devices  13.3 us (3%)
  other arithmetic  6.47 us (1%)
    all_to_all x1, blocking collectives, show_table_here(): all_to_all(current_arr, axis_name='tp', split_axis=array_dim, concat_axis...  191 us
    all_to_all x1, waiting for transfers between devices, on_device(): lax.all_to_all(partial_value, 'tp', split_axis=0, concat_axis=0, tiled=True)  141 us
    all_to_all x1, blocking collectives, on_device(): lax.all_to_all(slot_rows, 'ep', split_axis=0, concat_axis=0, tiled=True)  30.7 us
    all_to_all x1, waiting for transfers between devices, on_device(): lax.all_to_all(summed, 'ep', split_axis=0, concat_axis=0, tiled=True)  17.5 us
    dot_general x1, matrix products, on_device(): jnp.einsum('aecf,efd->aecd', hidden_units, down_weight, preferred_element...  16.6 us
    reshape x1, local copies, waits for them, and re-layouts, on_device(): partial_value.reshape(tp_size, ep_size * local_experts * capacity, -1)  16.3 us
    convert_element_type x1, local copies, waits for them, and re-layouts, on_device(): partial_value = jnp.einsum('aecf,efd->aecd', hidden_units, down_weight, p...  11.4 us
  transfers between devices with their start and end apart: 4, of which 3 were waited for; matrix products, arithmetic and copies ran while one was open for 2% of the time, Pallas kernels for 0%

profile of v1, /device:TPU:24, one launch (start us, length us, event | category | flops | bytes accessed | tf_op | source)
XLA Modules:
  0.0 482.6 jit_solution(5891827594901361238)
XLA Ops:
  7.2 0.8 copy.42
  8.3 0.2 select_reduce_fusion
  8.5 0.1 eq.72
  8.6 0.4 fusion.36
  8.9 1.0 fusion.60
  10.0 1.2 fusion.6
  11.2 0.3 copy.46
  11.6 30.7 %all_to_all.20 = bf16[32,1,3,2048]{3,2,1,0:T(4,128)(2,1)S(1)} all-to-all(bf16[32,1,3,2048]{3,2,1,0:T(4,128)(2,1)S(1)} %copy.46), channel_id=1, replica_groups=mesh['ep'=32,'tp'=16] {'ep'}, dimensions={0} | all-to-all | bytes 786432 | tf_op jit(solution)/shard_map/all_to_all | solution.py:159
  42.3 0.2 constant_dynamic-update-slice_fusion.15
  42.5 0.3 constant_dynamic-update-slice_fusion.14
  42.8 0.3 constant_dynamic-update-slice_fusion.13
  43.1 0.3 constant_dynamic-update-slice_fusion.12
  43.4 0.3 constant_dynamic-update-slice_fusion.11
  43.7 0.3 constant_dynamic-update-slice_fusion.10
  43.9 0.3 constant_dynamic-update-slice_fusion.9
  44.2 0.3 constant_dynamic-update-slice_fusion.8
  44.5 0.3 constant_dynamic-update-slice_fusion.7
  44.8 0.3 constant_dynamic-update-slice_fusion.6
  45.1 0.3 constant_dynamic-update-slice_fusion.5
  45.3 0.3 constant_dynamic-update-slice_fusion.4
  45.6 0.3 constant_dynamic-update-slice_fusion.3
  45.9 0.3 constant_dynamic-update-slice_fusion.2
  46.2 0.3 constant_dynamic-update-slice_fusion.1
  46.5 0.3 constant_dynamic-update-slice_fusion
  46.8 190.8 %all_to_all.21 = bf16[512,1,3,2048]{3,2,1,0:T(4,128)(2,1)S(1)} all-to-all(bf16[512,1,3,2048]{3,2,1,0:T(4,128)(2,1)S(1)} %constant_dynamic-update-slice_fusion), channel_id=1, replica_groups=mesh['ep'=32,'tp'=16] {'tp'}, dimensions={0} | all-to-all | bytes 12582912 | tf_op jit(solution)/shard_map/all_to_all | solution.py:18
  237.5 3.2 copy-done.1
  240.8 6.9 %fusion.25 = f32[512,1,3,128]{3,0,2,1:T(8,128)S(1)} fusion(bf16[512,1,3,2048]{3,2,1,0:T(4,128)(2,1)S(1)} %all_to_all.21, bf16[1,2048,128]{2,1,0:T(8,128)(2,1)S(1)} %copy-done.8), kind=kOutput, calls=%fused_computation.21 | convolution fusion | flops 805502976 | bytes 7602176 | tf_op jit(solution)/shard_map/aecd,edf->aecf/dot_general | solution.py:110
  247.7 16.6 %convert_bitcast_fusion = bf16[512,1,3,2048]{3,0,2,1:T(8,128)(2,1)} fusion(bf16[512,1,3,2048]{3,2,1,0:T(4,128)(2,1)} %copy-done.1, f32[512,1,3,128]{3,0,2,1:T(8,128)S(1)} %fusion.25, bf16[1,128,2048]{2,1,0:T(8,128)(2,1)S(1)} %copy-done.9, bf16[1,2048,128]{2,1,0:T(8,128)(2,1)S(1)} %copy-done.10), kind=kOutput, calls=%fused_computation.4 | convolution fusion | flops 1615527936 | bytes 14417920 | tf_op jit(solution)/shard_map/aecf,efd->aecd/dot_general | solution.py:161
  264.3 11.4 %copy.48 = bf16[512,1,3,2048]{3,2,0,1:T(4,128)(2,1)} copy(bf16[512,1,3,2048]{3,0,2,1:T(8,128)(2,1)} %convert_bitcast_fusion) | data formatting | bytes 12582912 | tf_op jit(solution)/shard_map/convert_element_type | solution.py:163
  275.7 16.3 %reshape.224 = bf16[16,96,2048]{2,1,0:T(8,128)(2,1)} reshape(bf16[512,1,3,2048]{3,2,0,1:T(4,128)(2,1)} %copy.48) | data formatting | bytes 12582912 | tf_op jit(solution)/shard_map/reshape | solution.py:164
  292.1 5.6 %all-to-all-start.2 = ((bf16[16,96,2048]{2,1,0:T(8,128)(2,1)}), bf16[16,96,2048]{2,1,0:T(8,128)(2,1)}, u32[]{:S(2)}, u32[]{:S(2)}) async-start(bf16[16,96,2048]{2,1,0:T(8,128)(2,1)} %reshape.224), calls=%async_computation.3 | async-start | bytes 12582912 | tf_op jit(solution)/shard_map/all_to_all | solution.py:165
  297.7 0.3 reduce-scatter.2.cloned.1.call-start
  298.2 2.8 collective-permute-start
  301.2 0.2 not_and_fusion
  301.4 0.1 reshape.213
  301.6 0.9 collective-permute-done
  302.6 0.5 fusion.107
  303.1 0.2 fusion.8
  303.5 0.4 fusion.35
  303.8 0.2 copy.41
  304.0 2.1 convolution_convert_fusion
  306.1 140.8 %all-to-all-done.2 = bf16[16,96,2048]{2,1,0:T(8,128)(2,1)} async-done(((bf16[16,96,2048]{2,1,0:T(8,128)(2,1)}), bf16[16,96,2048]{2,1,0:T(8,128)(2,1)}, u32[]{:S(2)}, u32[]{:S(2)}) %all-to-all-start.2) | async-done | bytes 6291488 | tf_op jit(solution)/shard_map/all_to_all | solution.py:165
  446.9 4.1 reduce_sum.76
  451.0 1.0 reshape.225
  452.0 4.6 all-to-all-start.3
  456.8 0.4 fusion.86
  457.2 17.5 %all-to-all-done.3 = bf16[32,3,2048]{2,1,0:T(4,128)(2,1)S(1)} async-done(((bf16[32,3,2048]{2,1,0:T(4,128)(2,1)}), bf16[32,3,2048]{2,1,0:T(4,128)(2,1)S(1)}, u32[]{:S(2)}, u32[]{:S(2)}) %all-to-all-start.3) | async-done | bytes 393248 | tf_op jit(solution)/shard_map/all_to_all | solution.py:168
  474.7 1.1 fusion.7
  (55 shorter events, 1.1 us)
Async XLA Ops:
  7.2 296.8 %copy-start = (bf16[192,2048]{1,0:T(8,128)(2,1)S(1)}, bf16[192,2048]{1,0:T(8,128)(2,1)}, u32[]{:S(2)}) copy-start(bf16[192,2048]{1,0:T(8,128)(2,1)} %param.20) | copy-start | bytes 2359300
  46.8 194.0 %copy-start.8 = (bf16[1,2048,128]{2,1,0:T(8,128)(2,1)S(1)}, bf16[1,2048,128]{2,1,0:T(8,128)(2,1)}, u32[]{:S(2)}) copy-start(bf16[1,2048,128]{2,1,0:T(8,128)(2,1)} %param.25) | copy-start | bytes 1572868
  237.5 3.2 copy-start.1
  240.8 6.9 %copy-start.9 = (bf16[1,128,2048]{2,1,0:T(8,128)(2,1)S(1)}, bf16[1,128,2048]{2,1,0:T(8,128)(2,1)}, u32[]{:S(2)}) copy-start(bf16[1,128,2048]{2,1,0:T(8,128)(2,1)} %param.27) | copy-start | bytes 1572868
  240.8 6.9 %copy-start.10 = (bf16[1,2048,128]{2,1,0:T(8,128)(2,1)S(1)}, bf16[1,2048,128]{2,1,0:T(8,128)(2,1)}, u32[]{:S(2)}) copy-start(bf16[1,2048,128]{2,1,0:T(8,128)(2,1)} %param.26) | copy-start | bytes 1572868
  292.0 5.9 %copy-start.3 = (bf16[512,64]{0,1:T(8,128)(2,1)S(1)}, bf16[512,64]{0,1:T(8,128)(2,1)}, u32[]{:S(2)}) copy-start(bf16[512,64]{0,1:T(8,128)(2,1)} %param.15) | copy-start | bytes 196612
  292.0 6.0 %copy-start.6 = (f32[1,64]{1,0:T(1,128)S(1)}, f32[1,64]{1,0:T(1,128)}, u32[]{:S(2)}) copy-start(f32[1,64]{1,0:T(1,128)} %param.18) | copy-start | bytes 772
  292.0 6.1 %copy-start.4 = (bf16[512,64]{0,1:T(8,128)(2,1)S(1)}, bf16[512,64]{0,1:T(8,128)(2,1)}, u32[]{:S(2)}) copy-start(bf16[512,64]{0,1:T(8,128)(2,1)} %param.16) | copy-start | bytes 196612
  292.0 8.9 %copy-start.2 = (bf16[512,192]{0,1:T(8,128)(2,1)S(1)}, bf16[512,192]{0,1:T(8,128)(2,1)}, u32[]{:S(2)}) copy-start(bf16[512,192]{0,1:T(8,128)(2,1)} %param.14) | copy-start | bytes 589828
  292.0 10.5 %copy-start.11 = (f32[3,64]{1,0:T(4,128)S(1)}, f32[3,64]{1,0:T(4,128)}, u32[]{:S(2)}) copy-start(f32[3,64]{1,0:T(4,128)} %param.17) | copy-start | bytes 2308
  292.1 11.0 %copy-start.7 = (f32[3]{0:T(128)S(1)}, f32[3]{0:T(128)}, u32[]{:S(2)}) copy-start(f32[3]{0:T(128)} %param.19) | copy-start | bytes 40
  292.1 154.8 %all-to-all-start.2 = ((bf16[16,96,2048]{2,1,0:T(8,128)(2,1)}), bf16[16,96,2048]{2,1,0:T(8,128)(2,1)}, u32[]{:S(2)}, u32[]{:S(2)}) async-start(bf16[16,96,2048]{2,1,0:T(8,128)(2,1)} %reshape.224), calls=%async_computation.3 | async-start | bytes 12582912 | tf_op jit(solution)/shard_map/all_to_all | solution.py:165
  297.7 178.1 %reduce-scatter.2.cloned.1.call-start = ((), (), s32[]{:S(2)}) async-start(), calls=%async_computation.5 | async-start | bytes 2228224 | tf_op jit(solution)/shard_map/reduce_scatter | solution.py:134
  298.2 4.4 collective-permute-start
  303.4 153.3 %copy-start.5 = (f32[32,2]{0,1:T(2,128)S(1)}, f32[32,2]{0,1:T(2,128)}, u32[]{:S(2)}) copy-start(f32[32,2]{0,1:T(2,128)} %param.24) | copy-start | bytes 772
  452.0 22.7 %all-to-all-start.3 = ((bf16[32,3,2048]{2,1,0:T(4,128)(2,1)}), bf16[32,3,2048]{2,1,0:T(4,128)(2,1)S(1)}, u32[]{:S(2)}, u32[]{:S(2)}) async-start(bf16[32,3,2048]{2,1,0:T(4,128)(2,1)} %reshape.225), calls=%async_computation.4 | async-start | bytes 1048576 | tf_op jit(solution)/shard_map/all_to_all | solution.py:168
Sparse Core Ops, SparseCore 0:
  306.3 131.9 reduce-scatter.1
